TPU v7x, 32 devices: a whole 2x2x4 slice. The times are simulated.
32 devices in a mesh: ep: 8 (over z, y), tp: 4 (over x, core).
Axes of the slice: x: 2, y: 2, z: 4, core: 2. Of those that a mesh axis runs over, the one named last changes fastest.
Arguments:
- queries: bfloat16 [4096, 2048], P('ep', 'tp'), may hold values from -6 to 6
- forget_pre: float32 [4096, 2048], P('ep', 'tp'), may hold values from -8 to 20
- value_in: bfloat16 [4096, 2048], P('ep', 'tp'), may hold values from -6 to 6
- out_gate: bfloat16 [4096, 2048], P('ep', 'tp'), may hold values from -6 to 6
- lower_bound: float32 [2048], P('tp'), may hold values from 0.5 to 0.8
- out_gain: float32 [128], replicated, may hold values from 0.1 to 1.9
- out_weight: bfloat16 [2048, 2048], P('tp'), may hold values from -0.125 to 0.125
- moe_tokens: bfloat16 [2048, 2048], P('ep'), may hold values from -6 to 6
- moe_gain: float32 [2048], replicated, may hold values from 0.1 to 1.9
- expert_ids: int32 [2048, 4], P('ep'), may hold values from 0 to 15, all different within a row; in each aligned block of 64 rows (0 to 63, 64 to 127, ...) at most 32 rows name the same one
- route_weights: float32 [2048, 4], P('ep'), may hold values from 0.1 to 1
- w_gate: bfloat16 [16, 2048, 1024], P('ep', None, 'tp'), may hold values from -0.125 to 0.125
- w_up: bfloat16 [16, 2048, 1024], P('ep', None, 'tp'), may hold values from -0.125 to 0.125
- w_down: bfloat16 [16, 1024, 2048], P('ep', 'tp'), may hold values from -0.1875 to 0.1875
Outputs:
- mixer_out: bfloat16 [4096, 2048], P(('ep', 'tp'))
- expert_out: bfloat16 [2048, 2048], P(('ep', 'tp'))
Inputs may be any that keep to these rules, and one draw needn't show every extreme that they name: `expert_ids`: each row names 4 different experts. In each aligned block of 64 rows no expert is named by more than 32 rows, and in some block some expert is named by exactly 32 rows.
All inputs are finite; a program needn't handle non-finite values.
Results may differ from a plain program's by a relative error of at most 0.01065.
Values may be sent and summed in bfloat16 or wider, within the bound.
A program may use at most 128 MiB of HBM per device.

v0:
```python
import jax
import jax.numpy as jnp
from jax import lax
from jax.sharding import PartitionSpec as P

HEAD_DIM = 128
BLOCK = 64


EPS = 1e-06
HIGHEST = lax.Precision.HIGHEST


def prefix(part, axis, combine, identity):
    place = lax.axis_index(axis)
    gathered = jax.tree.map(lambda a: lax.all_gather(a, axis), part)
    state = jax.tree.map(lambda a, e: jnp.zeros_like(a) + jnp.asarray(e, a.dtype), part, identity)

    def one(hop, state):
        return combine(
            state, jax.tree.map(lambda a: lax.dynamic_index_in_dim(a, hop, 0, False), gathered)
        )

    return lax.fori_loop(0, place, one, state)


def rms_scale(values, gain):
    return values * lax.rsqrt(jnp.mean(values * values, axis=-1, keepdims=True) + EPS) * gain


def block_step(memory, inputs):
    queries_block, weight_block, values_block, forget_block = inputs
    cumulative = jnp.cumsum(forget_block, axis=1)
    length = queries_block.shape[1]
    causal = (
        jnp.arange(length, dtype=jnp.int32)[:, None] >= jnp.arange(length, dtype=jnp.int32)[None, :]
    )
    decayed_query = queries_block * jnp.exp(cumulative)
    decayed_key = weight_block * jnp.exp(-cumulative)
    carried_out = jnp.einsum("htd,hde->hte", decayed_query, memory, precision=HIGHEST)
    scores = jnp.einsum("htd,hsd->hts", decayed_query, decayed_key, precision=HIGHEST)
    scores = jnp.where(causal[None], scores, 0.0)
    local_out = jnp.einsum("hts,hse->hte", scores, values_block, precision=HIGHEST)
    block_total = cumulative[:, -1:, :]
    added = jnp.einsum(
        "hsd,hse->hde",
        weight_block * jnp.exp(block_total - cumulative),
        values_block,
        precision=HIGHEST,
    )
    memory = jnp.exp(block_total[:, 0, :])[:, :, None] * memory + added
    return (memory, carried_out + local_out)


def to_blocks(array, head_count):
    row_count = array.shape[0]
    return (
        array.astype(jnp.float32)
        .reshape(row_count // BLOCK, BLOCK, head_count, HEAD_DIM)
        .transpose(0, 2, 1, 3)
    )


def combine_memory(earlier, later):
    return (earlier[0] * later[0], later[0][:, :, None] * earlier[1] + later[1])


def slot_ranks(ids_block, expert_count):
    onehot = (
        ids_block[:, :, None] == jnp.arange(expert_count, dtype=jnp.int32)[None, None, :]
    ).astype(jnp.int32)
    return jnp.sum(onehot * (jnp.cumsum(onehot, axis=1) - 1), axis=2)


def local(
    queries,
    forget_pre,
    value_in,
    out_gate,
    lower_bound,
    out_gain,
    out_weight,
    moe_tokens,
    moe_gain,
    expert_ids,
    route_weights,
    w_gate,
    w_up,
    w_down,
):
    lanes = lax.axis_size("tp")
    lane_index = lax.axis_index("tp")
    ep_count = lax.axis_size("ep")
    seq_rows, local_width = queries.shape
    model_width = out_weight.shape[1]
    head_count = local_width // HEAD_DIM
    weight_in = (1.0 - lower_bound) * jax.nn.sigmoid(-forget_pre)
    log_forget = jnp.log1p(-weight_in)
    cumulative = jnp.cumsum(log_forget, axis=0)
    span_total = cumulative[-1]
    to_end = (weight_in * jnp.exp(span_total[None, :] - cumulative)).reshape(
        seq_rows, head_count, HEAD_DIM
    )
    values_float = value_in.astype(jnp.float32).reshape(seq_rows, head_count, HEAD_DIM)
    local_memory = jnp.einsum("shd,she->hde", to_end, values_float, precision=HIGHEST)
    decay_total = jnp.exp(span_total).reshape(head_count, HEAD_DIM)
    neutral = (jnp.ones_like(decay_total), jnp.zeros_like(local_memory))
    earlier_part = prefix((decay_total, local_memory), "ep", combine_memory, neutral)
    final_memory, outputs = lax.scan(
        block_step,
        earlier_part[1],
        (
            to_blocks(queries, head_count),
            to_blocks(weight_in, head_count),
            to_blocks(value_in, head_count),
            to_blocks(log_forget, head_count),
        ),
    )
    outputs = outputs.transpose(0, 2, 1, 3).reshape(seq_rows, head_count, HEAD_DIM)
    gate_act = jax.nn.silu(out_gate.astype(jnp.float32)).reshape(seq_rows, head_count, HEAD_DIM)
    gated = (
        (rms_scale(outputs, out_gain) * gate_act)
        .reshape(seq_rows, local_width)
        .astype(jnp.bfloat16)
    )
    qrows = moe_tokens.shape[0] // lanes
    top_count = expert_ids.shape[1]
    local_experts = w_gate.shape[0]
    expert_count = local_experts * ep_count
    capacity = max(2, 2 * qrows * top_count // expert_count)
    send_tokens = lax.dynamic_slice_in_dim(moe_tokens, lane_index * qrows, qrows, 0)
    send_ids = lax.dynamic_slice_in_dim(expert_ids, lane_index * qrows, qrows, 0)
    quarters = send_tokens.shape[0] // qrows
    normed = rms_scale(send_tokens.astype(jnp.float32), moe_gain).astype(jnp.bfloat16)
    ids_block = send_ids.reshape(quarters, qrows * top_count)
    ranks = slot_ranks(ids_block, expert_count)
    quarter_base = jnp.arange(quarters, dtype=jnp.int32)[:, None] * (expert_count * capacity)
    slot_index = (quarter_base + ids_block * capacity + ranks).reshape(-1)
    source_row = jnp.arange(quarters * qrows * top_count, dtype=jnp.int32) // top_count
    sources = (
        jnp.full((quarters * expert_count * capacity,), quarters * qrows, jnp.int32)
        .at[slot_index]
        .set(source_row)
    )
    padded = jnp.concatenate([normed, jnp.zeros((1, model_width), jnp.bfloat16)], axis=0)
    outgoing = padded[sources].reshape(quarters, ep_count, local_experts * capacity, model_width)
    arrived = lax.all_to_all(outgoing, "ep", split_axis=1, concat_axis=1, tiled=True)
    piece = lax.all_gather(arrived, "tp", axis=0, tiled=True)
    shaped = piece.reshape(piece.shape[0], ep_count, local_experts, capacity, model_width)
    gate_pre = jnp.einsum("qsecd,edf->qsecf", shaped, w_gate, preferred_element_type=jnp.float32)
    up_pre = jnp.einsum("qsecd,edf->qsecf", shaped, w_up, preferred_element_type=jnp.float32)
    hidden = (jax.nn.silu(gate_pre) * up_pre).astype(jnp.bfloat16)
    lane_rows = ep_count * local_experts * capacity
    mixer_sum = lax.psum_scatter(
        jnp.dot(gated, out_weight, preferred_element_type=jnp.float32).astype(jnp.bfloat16),
        "tp",
        scatter_dimension=0,
        tiled=True,
    )
    projected = jnp.einsum("qsecf,efd->qsecd", hidden, w_down, preferred_element_type=jnp.float32)
    expert_sum = lax.psum_scatter(
        projected.reshape(lax.axis_size("tp") * lane_rows, model_width).astype(jnp.bfloat16),
        "tp",
        scatter_dimension=0,
        tiled=True,
    )
    leaving = expert_sum.reshape(ep_count, local_experts * capacity, model_width)
    returned = lax.all_to_all(leaving, "ep", split_axis=0, concat_axis=0, tiled=True)
    returned = returned.reshape(expert_count * capacity, model_width)
    own_quarter = lane_index * (quarters // lanes)
    own_ids = lax.dynamic_index_in_dim(ids_block, own_quarter, 0, keepdims=False)
    own_ranks = lax.dynamic_index_in_dim(ranks, own_quarter, 0, keepdims=False)
    picked = (
        returned[own_ids * capacity + own_ranks]
        .astype(jnp.float32)
        .reshape(qrows, top_count, model_width)
    )
    own_weights = lax.dynamic_slice_in_dim(route_weights, lane_index * qrows, qrows, 0)
    expert_out = jnp.sum(picked * own_weights[:, :, None], axis=1).astype(jnp.bfloat16)
    return (mixer_sum, expert_out)


def solution(mesh):
    in_specs = (
        P("ep", "tp"),
        P("ep", "tp"),
        P("ep", "tp"),
        P("ep", "tp"),
        P("tp"),
        P(),
        P("tp", None),
        P("ep", None),
        P(),
        P("ep", None),
        P("ep", None),
        P("ep", None, "tp"),
        P("ep", None, "tp"),
        P("ep", "tp", None),
    )
    out_specs = (P(("ep", "tp"), None), P(("ep", "tp"), None))
    return jax.shard_map(local, mesh=mesh, in_specs=in_specs, out_specs=out_specs, check_vma=False)
```

profile of v0, /device:TPU:0, one launch (start us, length us, event | category | flops | bytes accessed | tf_op | source)
XLA Modules:
  0.0 324.8 jit_solution(6466362243241929309)
XLA Ops:
  7.2 0.9 broadcast_multiply_fusion
  8.4 0.6 reduce-window.16
  9.6 1.4 scatter_custom_fusion
  11.1 1.1 fusion.36
  12.2 1.1 fusion.38
  13.3 3.3 %gather_fusion = bf16[512,2048]{1,0:T(8,128)(2,1)} fusion(bf16[65,2048]{1,0:T(8,128)(2,1)S(1)} %concatenate.3, s32[1024]{0:T(1024)S(1)} %pad_clamp_fusion.1), kind=kCustom, calls=%fused_computation | custom fusion | bytes 4196352 | tf_op jit(solution)/shard_map/gather | solution.py:146
  16.7 55.6 %all_to_all.10 = bf16[1,8,64,2048]{3,2,0,1:T(8,128)(2,1)} all-to-all(bf16[1,8,64,2048]{3,2,0,1:T(8,128)(2,1)} %bitcast.171), channel_id=1, replica_groups=mesh['ep'=8,'tp'=4] {'ep'}, dimensions={1} | all-to-all | bytes 4194304 | tf_op jit(solution)/shard_map/all_to_all | solution.py:147
  72.4 0.6 copy-done.6
  73.0 2.8 negate_log-plus-one_fusion
  75.8 0.7 fusion.33
  76.5 1.0 copy-done.4
  77.5 1.5 broadcast_add_fusion
  79.4 1.2 exponential_multiply_fusion
  80.6 2.6 copy.104
  83.3 2.8 fusion.40
  86.3 43.4 %all-gather.4.cloned.1.call-done = bf16[4,8,64,2048]{3,2,1,0:T(8,128)(2,1)} async-done(((bf16[1,8,64,2048]{3,2,1,0:T(8,128)(2,1)}), bf16[4,8,64,2048]{3,2,1,0:T(8,128)(2,1)}) %all-gather.4.cloned.1.call-update) | async-done | bytes 8388624 | tf_op jit(solution)/shard_map/all_gather | solution.py:148
  129.8 6.5 %fusion.15 = f32[2,4,8,32,256]{4,3,2,1,0:T(8,128)S(1)} fusion(bf16[4,8,2,32,2048]{4,3,2,1,0:T(8,128)(2,1)} %bitcast.199, bf16[2,2048,256]{2,1,0:T(8,128)(2,1)} %param.29), kind=kOutput, calls=%fused_computation.31 | convolution fusion | flops 2147483648 | bytes 12582912 | tf_op jit(solution)/shard_map/qsecd,edf->qsecf/dot_general | solution.py:150
  136.3 0.5 copy-done.10
  136.7 2.6 fusion.20
  139.4 5.6 %convert_bitcast_fusion = bf16[4,8,2,32,2048]{4,3,1,0,2:T(8,128)(2,1)} fusion(bf16[4,8,2,32,256]{4,3,1,0,2:T(8,128)(2,1)S(1)} %fusion.20, bf16[2,256,2048]{2,1,0:T(8,128)(2,1)S(1)} %copy-done), kind=kOutput, calls=%fused_computation.28 | convolution fusion | flops 2151677952 | bytes 11534336 | tf_op jit(solution)/shard_map/qsecf,efd->qsecd/dot_general | solution.py:160
  144.9 8.3 %copy.99 = bf16[4,8,2,32,2048]{4,3,2,1,0:T(8,128)(2,1)} copy(bf16[4,8,2,32,2048]{4,3,1,0,2:T(8,128)(2,1)} %convert_bitcast_fusion) | data formatting | bytes 16777216 | tf_op jit(solution)/shard_map/convert_element_type | solution.py:162
  153.3 1.3 reshape.281
  155.1 1.3 reshape.297
  156.4 2.4 reshape.298
  158.8 26.6 %all_gather.12 = f32[8,4,128]{2,1,0:T(4,128)S(1)} all-gather(f32[1,4,128]{2,1,0:T(4,128)S(1)} %bitcast.193), channel_id=1, replica_groups=mesh['ep'=8,'tp'=4] {'ep'}, dimensions={0}, use_global_device_ids=true | all-gather | bytes 18432 | tf_op jit(solution)/shard_map/all_gather | solution.py:16
  185.7 30.8 %while.25 = (s32[]{:T(128)}, f32[4,128,128]{2,1,0:T(8,128)S(1)}, f32[8,4,64,128]{3,2,1,0:T(8,128)S(1)}, f32[8,4,64,128]{3,1,2,0:T(4,128)}, f32[8,4,64,128]{3,1,2...) while((s32[]{:T(128)}, f32[4,128,128]{2,1,0:T(8,128)S(1)}, ...), condition=%wide.region_6.7_spmd, body=%wide.region_4.6_spmd.sunk | while | flops 153440256 | bytes 4083821 | solution.py:109
  185.7 0.9 constant_dynamic-slice_fusion.9
  186.8 1.0 constant_dynamic-slice_fusion.10
  188.4 0.4 fusion.73
  188.8 0.7 convolution_add_fusion.3
  189.5 0.9 constant_dynamic-slice_fusion.9
  190.6 1.1 constant_dynamic-slice_fusion.10
  192.4 0.4 fusion.73
  192.8 0.7 convolution_add_fusion.3
  193.5 1.0 constant_dynamic-slice_fusion.9
  194.6 1.1 constant_dynamic-slice_fusion.10
  196.3 0.4 fusion.73
  196.7 0.7 convolution_add_fusion.3
  197.4 0.9 constant_dynamic-slice_fusion.9
  198.5 1.0 constant_dynamic-slice_fusion.10
  200.1 0.4 fusion.73
  200.5 0.7 convolution_add_fusion.3
  201.2 0.9 constant_dynamic-slice_fusion.9
  202.3 1.0 constant_dynamic-slice_fusion.10
  203.9 0.4 fusion.73
  204.3 0.7 convolution_add_fusion.3
  205.0 1.0 constant_dynamic-slice_fusion.9
  206.1 1.1 constant_dynamic-slice_fusion.10
  208.2 0.7 convolution_add_fusion.3
  208.9 0.9 constant_dynamic-slice_fusion.9
  210.0 1.0 constant_dynamic-slice_fusion.10
  212.1 0.7 convolution_add_fusion.3
  212.7 0.9 constant_dynamic-slice_fusion.9
  213.8 1.0 constant_dynamic-slice_fusion.10
  215.9 0.7 convolution_add_fusion.3
  217.1 0.7 copy.87
  217.8 0.6 mul.147
  218.4 4.3 %convolution_convert_fusion = bf16[512,2048]{1,0:T(8,128)(2,1)} fusion(bf16[512,2048]{1,0:T(8,128)(2,1)} %param.24, bf16[512,512]{1,0:T(8,128)(2,1)S(1)} %copy-done.11, f32[64,8,4,128]{3,2,1,0:T(4,128)S(1)} %bitcast.183, f32[64,8,4,128]{3,2,1,0:T(4,128)S(1)} %bitcast.185, f32[512]{0:T(512)S(1)} %broadcast_bitcast_fusion), kind=kOutput, calls=%fused_computation.33 | convolution fusion | flops 1077149696 | bytes 6817792 | tf_op jit(solution)/shard_map/dot_general | solution.py:155
  222.7 31.7 %reduce-scatter.5.cloned.1.call-done = bf16[512,2048]{1,0:T(8,128)(2,1)} async-done(((bf16[2048,2048]{1,0:T(8,128)(2,1)}), bf16[512,2048]{1,0:T(8,128)(2,1)}) %reduce-scatter.5.cloned.1.call-update) | async-done | bytes 2097168 | tf_op jit(solution)/shard_map/reduce_scatter | solution.py:161
  254.4 5.7 %all-to-all-start.1 = ((bf16[8,64,2048]{2,1,0:T(8,128)(2,1)}), bf16[8,64,2048]{2,1,0:T(8,128)(2,1)}, u32[]{:S(2)}, u32[]{:S(2)}) async-start(bf16[8,64,2048]{2,1,0:T(8,128)(2,1)} %bitcast.182), calls=%async_computation.3 | async-start | bytes 4194304 | tf_op jit(solution)/shard_map/all_to_all | solution.py:168
  260.2 48.0 %all-to-all-done.1 = bf16[8,64,2048]{2,1,0:T(8,128)(2,1)} async-done(((bf16[8,64,2048]{2,1,0:T(8,128)(2,1)}), bf16[8,64,2048]{2,1,0:T(8,128)(2,1)}, u32[]{:S(2)}, u32[]{:S(2)}) %all-to-all-start.1) | async-done | bytes 2097184 | tf_op jit(solution)/shard_map/all_to_all | solution.py:168
  308.2 4.4 %gather_fusion.1 = bf16[256,2048]{1,0:T(8,128)(2,1)S(1)} fusion(bf16[512,2048]{1,0:T(8,128)(2,1)} %bitcast.48, s32[1024]{0:T(1024)S(1)} %pad_clamp_fusion), kind=kCustom, calls=%fused_computation.1 | custom fusion | bytes 2098176 | tf_op jit(solution)/shard_map/gather | solution.py:174
  312.6 1.7 reshape.296
  314.3 3.9 %multiply_reduce_fusion = bf16[64,2048]{1,0:T(8,128)(2,1)} fusion(f32[64,4,2048]{2,1,0:T(4,128)} %reshape.296, f32[64,4]{1,0:T(8,128)S(1)} %copy.100), kind=kLoop, calls=%fused_computation.44 | loop fusion | flops 917504 | bytes 2360320 | tf_op jit(solution)/shard_map/reduce_sum | solution.py:179
  (127 shorter events, 10.5 us)
Async XLA Ops:
  7.2 132.2 %copy-start = (bf16[2,256,2048]{2,1,0:T(8,128)(2,1)S(1)}, bf16[2,256,2048]{2,1,0:T(8,128)(2,1)}, u32[]{:S(2)}) copy-start(bf16[2,256,2048]{2,1,0:T(8,128)(2,1)} %param.31) | copy-start | bytes 6291460
  7.2 122.6 %all-gather.4.cloned.1.call-start = ((), (), s32[]{:S(2)}) async-start(), calls=%async_computation.5 | async-start | bytes 10485760 | tf_op jit(solution)/shard_map/all_gather | solution.py:148
  72.3 0.7 copy-start.6
  72.4 113.1 %all-gather.6.cloned.1.call-start = ((), (), s32[]{:S(2)}) async-start(), calls=%async_computation.7 | async-start | bytes 2359296 | tf_op jit(solution)/shard_map/all_gather | solution.py:16
  76.5 1.0 copy-start.4
  77.5 1.9 copy-start.2
  86.1 168.3 %reduce-scatter.5.cloned.1.call-start = ((), (), s32[]{:S(2)}) async-start(), calls=%async_computation.6 | async-start | bytes 10485760 | tf_op jit(solution)/shard_map/reduce_scatter | solution.py:161
  129.8 6.5 %copy-start.9 = (bf16[4,8,64,2048]{3,2,1,0:T(8,128)(2,1)S(1)}, bf16[4,8,64,2048]{3,2,1,0:T(8,128)(2,1)}, u32[]{:S(2)}) copy-start(bf16[4,8,64,2048]{3,2,1,0:T(8,128)(2,1)} %all-gather.4.cloned.1.call-done) | copy-start | bytes 25165828
  129.8 7.0 %copy-start.10 = (bf16[2,2048,256]{2,1,0:T(8,128)(2,1)S(1)}, bf16[2,2048,256]{2,1,0:T(8,128)(2,1)}, u32[]{:S(2)}) copy-start(bf16[2,2048,256]{2,1,0:T(8,128)(2,1)} %param.30) | copy-start | bytes 6291460
  153.3 1.4 copy-start.3
  153.3 164.9 %reduce-scatter.3.cloned.1.call-start = ((), (), s32[]{:S(2)}) async-start(), calls=%async_computation.4 | async-start | bytes 2621440 | tf_op jit(solution)/shard_map/reduce_scatter | solution.py:154
  153.3 1.7 copy-start.5
  155.0 30.4 %copy-start.8 = (f32[128]{0:T(128)S(1)}, f32[128]{0:T(128)}, u32[]{:S(2)}) copy-start(f32[128]{0:T(128)} %param.23) | copy-start | bytes 1540
  216.9 1.5 copy-start.11
  254.4 5.7 %copy-start.7 = (f32[256,4]{0,1:T(4,128)S(1)}, f32[256,4]{0,1:T(4,128)}, u32[]{:S(2)}) copy-start(f32[256,4]{0,1:T(4,128)} %param.28) | copy-start | bytes 12292
  254.4 53.8 %all-to-all-start.1 = ((bf16[8,64,2048]{2,1,0:T(8,128)(2,1)}), bf16[8,64,2048]{2,1,0:T(8,128)(2,1)}, u32[]{:S(2)}, u32[]{:S(2)}) async-start(bf16[8,64,2048]{2,1,0:T(8,128)(2,1)} %bitcast.182), calls=%async_computation.3 | async-start | bytes 4194304 | tf_op jit(solution)/shard_map/all_to_all | solution.py:168
  308.2 10.0 %copy-start.1 = (bf16[2,256,2048]{2,1,0:T(8,128)(2,1)S(1)}, bf16[2,256,2048]{2,1,0:T(8,128)(2,1)}, u32[]{:S(2)}) copy-start(bf16[2,256,2048]{2,1,0:T(8,128)(2,1)} %param.31) | copy-start | bytes 6291460
Sparse Core Ops, SparseCore 0:
  72.5 57.2 all-gather.3
  132.5 49.1 all-gather.5
  184.3 70.0 reduce-scatter.4
  257.3 31.1 reduce-scatter.2
where the time goes:
time: 326 us; the launch traced here: 325 us
  waiting for transfers between devices  123 us (38%)
  blocking collectives  82.3 us (25%)
  local copies, waits for them, and re-layouts  47.9 us (15%)
  matrix products  34.9 us (11%)
  other arithmetic  15.5 us (5%)
  between operations  14.1 us (4%)
  starting transfers between devices  6 us (2%)
    all_to_all x1, blocking collectives, local(): lax.all_to_all(outgoing, 'ep', split_axis=1, concat_axis=1, tiled=True)  55.6 us
    all_to_all x1, waiting for transfers between devices, local(): lax.all_to_all(leaving, 'ep', split_axis=0, concat_axis=0, tiled=True)  48 us
    all_gather x1, waiting for transfers between devices, local(): piece = lax.all_gather(arrived, 'tp', axis=0, tiled=True)  43.4 us
    reduce_scatter x1, waiting for transfers between devices, local(): lax.psum_scatter(projected.reshape(lax.axis_size('tp') * lane_rows, model...  31.7 us
    all_gather x1, blocking collectives, prefix(): gathered = jax.tree.map(lambda a: lax.all_gather(a, axis), part)  26.6 us
    dynamic_slice x24, local copies, waits for them, and re-layouts, local(): lax.scan(block_step, earlier_part[1], (to_blocks(queries, head_count), to...  15.7 us
    convert_element_type x1, local copies, waits for them, and re-layouts, local(): projected.reshape(lax.axis_size('tp') * lane_rows, model_width)  8.31 us
  transfers between devices with their start and end apart: 5, of which 3 were waited for; matrix products, arithmetic and copies ran while one was open for 27% of the time, Pallas kernels for 0%

commit v1 on v0

--- a/solution.py
+++ b/solution.py
@@ -1,6 +1,8 @@
 import jax
 import jax.numpy as jnp
 from jax import lax
+from jax.experimental import pallas as pl
+from jax.experimental.pallas import tpu as pltpu
 from jax.sharding import PartitionSpec as P
 
 HEAD_DIM = 128
@@ -9,19 +11,6 @@
 
 EPS = 1e-06
 HIGHEST = lax.Precision.HIGHEST
-
-
-def prefix(part, axis, combine, identity):
-    place = lax.axis_index(axis)
-    gathered = jax.tree.map(lambda a: lax.all_gather(a, axis), part)
-    state = jax.tree.map(lambda a, e: jnp.zeros_like(a) + jnp.asarray(e, a.dtype), part, identity)
-
-    def one(hop, state):
-        return combine(
-            state, jax.tree.map(lambda a: lax.dynamic_index_in_dim(a, hop, 0, False), gathered)
-        )
-
-    return lax.fori_loop(0, place, one, state)
 
 
 def rms_scale(values, gain):
@@ -61,10 +50,6 @@
     )
 
 
-def combine_memory(earlier, later):
-    return (earlier[0] * later[0], later[0][:, :, None] * earlier[1] + later[1])
-
-
 def slot_ranks(ids_block, expert_count):
     onehot = (
         ids_block[:, :, None] == jnp.arange(expert_count, dtype=jnp.int32)[None, None, :]
@@ -72,57 +57,315 @@
     return jnp.sum(onehot * (jnp.cumsum(onehot, axis=1) - 1), axis=2)
 
 
-def local(
-    queries,
-    forget_pre,
-    value_in,
-    out_gate,
-    lower_bound,
-    out_gain,
-    out_weight,
-    moe_tokens,
-    moe_gain,
-    expert_ids,
-    route_weights,
-    w_gate,
-    w_up,
-    w_down,
+MESH = pl.DeviceIdType.MESH
+VMEM = pl.BlockSpec(memory_space=pltpu.VMEM)
+
+
+def ring_place(index, planes):
+    plane, side = index // 2, index % 2
+    return (1 - side) * plane + side * (2 * planes - 1 - plane)
+
+
+def ring_index(place, planes):
+    back = place // planes
+    return (1 - back) * 2 * place + back * ((2 * planes - 1 - place) * 2 + 1)
+
+
+def ring_setup(count):
+    planes = count // 2
+    index = lax.axis_index("ep")
+    lane = lax.axis_index("tp")
+    place = ring_place(index, planes)
+    right = ring_index((place + 1) % count, planes)
+    left = ring_index((place + count - 1) % count, planes)
+    core = lane % 2
+    partner = lane + 1 - 2 * core
+    return index, lane, core, (right, lane), (left, lane), (index, partner)
+
+
+def greet(devices):
+    barrier = pltpu.get_barrier_semaphore()
+    for device in devices:
+        pl.semaphore_signal(barrier, inc=1, device_id=device, device_id_type=MESH)
+    pl.semaphore_wait(barrier, len(devices))
+
+
+def remote(source, target, send, receive, device):
+    return pltpu.make_async_remote_copy(
+        src_ref=source,
+        dst_ref=target,
+        send_sem=send,
+        recv_sem=receive,
+        device_id=device,
+        device_id_type=MESH,
+    )
+
+
+def gather_kernel(
+    count, experts, width, own_ref, gate_ref, up_ref, down_ref, out_ref, held, send, recv, psend, precv
+):
+    index, lane, core, right, left, partner = ring_setup(count)
+    local_experts = gate_ref.shape[0]
+    half = held.shape[2]
+    turns = count // 2
+    greet((right, left, partner))
+
+    def part(side, turn):
+        if turn < turns:
+            return pl.ds(0, half)
+        return pl.ds(side * (half // 2), half // 2)
+
+    def slot(side, turn):
+        return turn if side == 0 else count - turn
+
+    def hop(side, turn):
+        rows = part(side, turn)
+        target = held.at[slot(side, turn), core, rows]
+        source = (
+            own_ref.at[core, rows] if turn == 1 else held.at[slot(side, turn - 1), core, rows]
+        )
+        return remote(
+            source, target, send.at[side, turn - 1], recv.at[side, turn - 1], (right, left)[side]
+        )
+
+    def across(side, turn):
+        piece = held.at[slot(side, turn), core, part(side, turn)]
+        return remote(piece, piece, psend.at[side, turn - 1], precv.at[side, turn - 1], partner)
+
+    def landed(side, turn):
+        piece = held.at[slot(side, turn), 1 - core, part(side, turn)]
+        return remote(piece, piece, psend.at[side, turn - 1], precv.at[side, turn - 1], partner)
+
+    def experts_of(block, place):
+        rows = block.shape[0]
+        tokens = block[:, :width]
+        extra = block[:, width:].astype(jnp.float32)
+        column = lax.broadcasted_iota(jnp.int32, extra.shape, 1)
+        hidden = []
+        for expert in range(local_experts):
+            number = index * local_experts + expert
+            chosen = (column == number) | (column == number + experts)
+            weight = jnp.sum(jnp.where(chosen, extra, 0.0), axis=1, keepdims=True)
+            gate = jnp.dot(tokens, gate_ref[expert], preferred_element_type=jnp.float32)
+            up = jnp.dot(tokens, up_ref[expert], preferred_element_type=jnp.float32)
+            hidden.append((jax.nn.silu(gate) * up * weight).astype(jnp.bfloat16))
+        total = jnp.dot(hidden[0], down_ref[0], preferred_element_type=jnp.float32)
+        for expert in range(1, local_experts):
+            total += jnp.dot(
+                hidden[expert], down_ref[expert], preferred_element_type=jnp.float32
+            )
+        for part_at in range(2):
+            out_ref[place, part_at] = total[part_at * half : (part_at + 1) * half].astype(
+                jnp.bfloat16
+            )
+
+    for side in range(2):
+        hop(side, 1).start()
+    experts_of(own_ref[...].reshape(2 * half, own_ref.shape[2]), 0)
+    for turn in range(1, turns + 1):
+        for side in range(2):
+            hop(side, turn).wait_recv()
+            if turn < turns:
+                hop(side, turn + 1).start()
+            across(side, turn).start()
+        for side in range(2):
+            landed(side, turn).wait_recv()
+        if turn < turns:
+
+            def body(step, carry):
+                place = turn + step * (count - 2 * turn)
+                experts_of(held[place].reshape(2 * half, held.shape[3]), place)
+                return carry
+
+            lax.fori_loop(0, 2, body, 0)
+        else:
+            experts_of(held[turn].reshape(2 * half, held.shape[3]), turn)
+    for turn in range(1, turns + 1):
+        for side in range(2):
+            hop(side, turn).wait_send()
+            across(side, turn).wait_send()
+
+
+def scatter_kernel(
+    count, part_ref, out_ref, total, other, came, final, crossed, send, recv, psend, precv, xsend, xrecv
+):
+    index, lane, core, right, left, partner = ring_setup(count)
+    half = part_ref.shape[2]
+    turns = count // 2
+    cross_at = lane // 2
+    cross = (index, lane + 2 - 4 * cross_at)
+    greet((right, left, partner, cross))
+    order = [turns]
+    for distance in range(turns - 1, 0, -1):
+        order += [count - distance, distance]
+    order += [0]
+
+    def swap(place):
+        return remote(
+            part_ref.at[place, 1 - core], other.at[place], psend.at[place], precv.at[place], partner
+        )
+
+    for place in order:
+        swap(place).start()
+
+    def settle(place):
+        swap(place).wait_recv()
+        total[place] = (
+            part_ref[place, core].astype(jnp.float32) + other[place].astype(jnp.float32)
+        ).astype(jnp.bfloat16)
+
+    def rows_of(side, turn):
+        if turn > 1:
+            return pl.ds(0, half)
+        return pl.ds(side * (half // 2), half // 2)
+
+    def hop(side, turn):
+        distance = turns - turn + 1
+        place = count - distance if side == 0 else distance
+        rows = rows_of(side, turn)
+        return remote(
+            total.at[place, rows],
+            came.at[side, turn - 1, rows],
+            send.at[side, turn - 1],
+            recv.at[side, turn - 1],
+            (right, left)[side],
+        )
+
+    settle(turns)
+    for side in range(2):
+        hop(side, 1).start()
+    for turn in range(1, turns):
+        distance = turns - turn
+        for side in range(2):
+            settle(count - distance if side == 0 else distance)
+        for side in range(2):
+            place = count - distance if side == 0 else distance
+            rows = rows_of(side, turn)
+            hop(side, turn).wait_recv()
+            total[place, rows] = (
+                total[place, rows].astype(jnp.float32)
+                + came[side, turn - 1, rows].astype(jnp.float32)
+            ).astype(jnp.bfloat16)
+            hop(side, turn + 1).start()
+    swap(0).wait_recv()
+    for side in range(2):
+        hop(side, turns).wait_recv()
+    summed = (
+        part_ref[0, core].astype(jnp.float32)
+        + other[0].astype(jnp.float32)
+        + came[0, turns - 1].astype(jnp.float32)
+        + came[1, turns - 1].astype(jnp.float32)
+    )
+    final[...] = summed.astype(jnp.bfloat16).reshape(final.shape)
+    over = remote(final.at[1 - cross_at], crossed, xsend, xrecv, cross)
+    over.start()
+    over.wait_recv()
+    out_ref[...] = (final[cross_at].astype(jnp.float32) + crossed[...].astype(jnp.float32)).astype(
+        jnp.bfloat16
+    )
+    over.wait_send()
+    for place in range(count):
+        swap(place).wait_send()
+    for turn in range(1, turns + 1):
+        for side in range(2):
+            hop(side, turn).wait_send()
+
+
+def dense_parts(normed, ids, weights, w_gate, w_up, w_down, ep_count):
+    rows, width = normed.shape
+    local_experts = w_gate.shape[0]
+    experts = local_experts * ep_count
+    half = rows // 2
+    routes = jnp.sum(
+        jnp.where(
+            ids[:, :, None] == jnp.arange(experts, dtype=jnp.int32)[None, None, :],
+            weights[:, :, None],
+            0.0,
+        ),
+        axis=1,
+    )
+    high = lax.reduce_precision(routes, 8, 7)
+    low = routes - high
+    margin = -(-2 * experts // 128) * 128
+    extra = jnp.concatenate(
+        [high, low, jnp.zeros((rows, margin - 2 * experts), jnp.float32)], axis=1
+    ).astype(jnp.bfloat16)
+    full = jnp.concatenate([normed, extra], axis=1)
+    stride = width + margin
+    full = full.reshape(2, 2, half // 2, stride).transpose(1, 0, 2, 3).reshape(2, half, stride)
+    turns = ep_count // 2
+    return full, margin, half, turns, experts
+
+
+def moe_gather(full, w_gate, w_up, w_down, ep_count, experts):
+    half, stride = full.shape[1:]
+    width = w_down.shape[2]
+    turns = ep_count // 2
+    sems = pltpu.SemaphoreType.DMA((2, turns))
+    rows = 2 * half * ep_count
+    flops = 2 * rows * w_gate.size * 3
+    return pl.pallas_call(
+        lambda *refs: gather_kernel(ep_count, experts, width, *refs),
+        out_shape=jax.ShapeDtypeStruct((ep_count, 2, half, width), jnp.bfloat16),
+        in_specs=[VMEM] * 4,
+        out_specs=VMEM,
+        scratch_shapes=[
+            pltpu.VMEM((ep_count, 2, half, stride), jnp.bfloat16),
+            sems,
+            sems,
+            sems,
+            sems,
+        ],
+        compiler_params=pltpu.CompilerParams(
+            collective_id=0, has_side_effects=True, vmem_limit_bytes=58 * 2**20
+        ),
+        cost_estimate=pl.CostEstimate(
+            flops=flops, bytes_accessed=100 * 2**20, transcendentals=0
+        ),
+        name="moe_gather",
+    )(full, w_gate, w_up, w_down)
+
+
+def moe_scatter(parts):
+    count, _, half, width = parts.shape
+    turns = count // 2
+    sems = pltpu.SemaphoreType.DMA((2, turns))
+    each = pltpu.SemaphoreType.DMA((count,))
+    block = (count, half, width)
+    return pl.pallas_call(
+        lambda *refs: scatter_kernel(count, *refs),
+        out_shape=jax.ShapeDtypeStruct((half // 2, width), jnp.bfloat16),
+        in_specs=[VMEM],
+        out_specs=VMEM,
+        scratch_shapes=[
+            pltpu.VMEM(block, jnp.bfloat16),
+            pltpu.VMEM(block, jnp.bfloat16),
+            pltpu.VMEM((2, turns, half, width), jnp.bfloat16),
+            pltpu.VMEM((2, half // 2, width), jnp.bfloat16),
+            pltpu.VMEM((half // 2, width), jnp.bfloat16),
+            sems,
+            sems,
+            each,
+            each,
+            pltpu.SemaphoreType.DMA,
+            pltpu.SemaphoreType.DMA,
+        ],
+        compiler_params=pltpu.CompilerParams(
+            collective_id=1, has_side_effects=True, vmem_limit_bytes=58 * 2**20
+        ),
+        cost_estimate=pl.CostEstimate(
+            flops=0, bytes_accessed=150 * 2**20, transcendentals=0
+        ),
+        name="moe_scatter",
+    )(parts)
+
+
+def sparse_experts(
+    moe_tokens, moe_gain, expert_ids, route_weights, w_gate, w_up, w_down, model_width
 ):
     lanes = lax.axis_size("tp")
     lane_index = lax.axis_index("tp")
     ep_count = lax.axis_size("ep")
-    seq_rows, local_width = queries.shape
-    model_width = out_weight.shape[1]
-    head_count = local_width // HEAD_DIM
-    weight_in = (1.0 - lower_bound) * jax.nn.sigmoid(-forget_pre)
-    log_forget = jnp.log1p(-weight_in)
-    cumulative = jnp.cumsum(log_forget, axis=0)
-    span_total = cumulative[-1]
-    to_end = (weight_in * jnp.exp(span_total[None, :] - cumulative)).reshape(
-        seq_rows, head_count, HEAD_DIM
-    )
-    values_float = value_in.astype(jnp.float32).reshape(seq_rows, head_count, HEAD_DIM)
-    local_memory = jnp.einsum("shd,she->hde", to_end, values_float, precision=HIGHEST)
-    decay_total = jnp.exp(span_total).reshape(head_count, HEAD_DIM)
-    neutral = (jnp.ones_like(decay_total), jnp.zeros_like(local_memory))
-    earlier_part = prefix((decay_total, local_memory), "ep", combine_memory, neutral)
-    final_memory, outputs = lax.scan(
-        block_step,
-        earlier_part[1],
-        (
-            to_blocks(queries, head_count),
-            to_blocks(weight_in, head_count),
-            to_blocks(value_in, head_count),
-            to_blocks(log_forget, head_count),
-        ),
-    )
-    outputs = outputs.transpose(0, 2, 1, 3).reshape(seq_rows, head_count, HEAD_DIM)
-    gate_act = jax.nn.silu(out_gate.astype(jnp.float32)).reshape(seq_rows, head_count, HEAD_DIM)
-    gated = (
-        (rms_scale(outputs, out_gain) * gate_act)
-        .reshape(seq_rows, local_width)
-        .astype(jnp.bfloat16)
-    )
     qrows = moe_tokens.shape[0] // lanes
     top_count = expert_ids.shape[1]
     local_experts = w_gate.shape[0]
@@ -151,12 +394,6 @@
     up_pre = jnp.einsum("qsecd,edf->qsecf", shaped, w_up, preferred_element_type=jnp.float32)
     hidden = (jax.nn.silu(gate_pre) * up_pre).astype(jnp.bfloat16)
     lane_rows = ep_count * local_experts * capacity
-    mixer_sum = lax.psum_scatter(
-        jnp.dot(gated, out_weight, preferred_element_type=jnp.float32).astype(jnp.bfloat16),
-        "tp",
-        scatter_dimension=0,
-        tiled=True,
-    )
     projected = jnp.einsum("qsecf,efd->qsecd", hidden, w_down, preferred_element_type=jnp.float32)
     expert_sum = lax.psum_scatter(
         projected.reshape(lax.axis_size("tp") * lane_rows, model_width).astype(jnp.bfloat16),
@@ -177,6 +414,90 @@
     )
     own_weights = lax.dynamic_slice_in_dim(route_weights, lane_index * qrows, qrows, 0)
     expert_out = jnp.sum(picked * own_weights[:, :, None], axis=1).astype(jnp.bfloat16)
+    return expert_out
+
+
+def local(
+    queries,
+    forget_pre,
+    value_in,
+    out_gate,
+    lower_bound,
+    out_gain,
+    out_weight,
+    moe_tokens,
+    moe_gain,
+    expert_ids,
+    route_weights,
+    w_gate,
+    w_up,
+    w_down,
+):
+    lanes = lax.axis_size("tp")
+    ep_count = lax.axis_size("ep")
+    seq_rows, local_width = queries.shape
+    model_width = out_weight.shape[1]
+    head_count = local_width // HEAD_DIM
+    weight_in = (1.0 - lower_bound) * jax.nn.sigmoid(-forget_pre)
+    log_forget = jnp.log1p(-weight_in)
+    cumulative = jnp.cumsum(log_forget, axis=0)
+    span_total = cumulative[-1]
+    to_end = (weight_in * jnp.exp(span_total[None, :] - cumulative)).reshape(
+        seq_rows, head_count, HEAD_DIM
+    )
+    values_float = value_in.astype(jnp.float32).reshape(seq_rows, head_count, HEAD_DIM)
+    local_memory = jnp.einsum("shd,she->hde", to_end, values_float, precision=HIGHEST)
+    decay_total = jnp.exp(span_total).reshape(head_count, HEAD_DIM)
+    packed = jnp.concatenate([local_memory, decay_total[:, None, :]], axis=1)
+    tokens, top_count = expert_ids.shape
+    dense_slots = 2 * (tokens // lanes) * top_count * lanes
+    dense = lanes == 4 and ep_count % 2 == 0 and tokens * ep_count <= dense_slots
+    if dense:
+        normed = rms_scale(moe_tokens.astype(jnp.float32), moe_gain).astype(jnp.bfloat16)
+        full, _, _, _, experts = dense_parts(
+            normed, expert_ids, route_weights, w_gate, w_up, w_down, ep_count
+        )
+        full, packed = lax.optimization_barrier((full, packed))
+    gathered = lax.all_gather(packed, "ep")
+    if dense:
+        parts = moe_gather(full, w_gate, w_up, w_down, ep_count, experts)
+        gathered, parts = lax.optimization_barrier((gathered, parts))
+    place = lax.axis_index("ep")
+
+    def one(hop, state):
+        block = lax.dynamic_index_in_dim(gathered, hop, 0, False)
+        return block[:, HEAD_DIM:, :].reshape(head_count, HEAD_DIM, 1) * state + block[:, :HEAD_DIM]
+
+    earlier_memory = lax.fori_loop(0, place, one, jnp.zeros_like(local_memory))
+    final_memory, outputs = lax.scan(
+        block_step,
+        earlier_memory,
+        (
+            to_blocks(queries, head_count),
+            to_blocks(weight_in, head_count),
+            to_blocks(value_in, head_count),
+            to_blocks(log_forget, head_count),
+        ),
+    )
+    outputs = outputs.transpose(0, 2, 1, 3).reshape(seq_rows, head_count, HEAD_DIM)
+    gate_act = jax.nn.silu(out_gate.astype(jnp.float32)).reshape(seq_rows, head_count, HEAD_DIM)
+    gated = (
+        (rms_scale(outputs, out_gain) * gate_act)
+        .reshape(seq_rows, local_width)
+        .astype(jnp.bfloat16)
+    )
+    mixer_part = jnp.dot(gated, out_weight, preferred_element_type=jnp.float32).astype(
+        jnp.bfloat16
+    )
+    if dense:
+        mixer_part, parts = lax.optimization_barrier((mixer_part, parts))
+    mixer_sum = lax.psum_scatter(mixer_part, "tp", scatter_dimension=0, tiled=True)
+    if dense:
+        expert_out = moe_scatter(parts)
+    else:
+        expert_out = sparse_experts(
+            moe_tokens, moe_gain, expert_ids, route_weights, w_gate, w_up, w_down, model_width
+        )
     return (mixer_sum, expert_out)
 
 

time: 326 us -> 241 us (0.74)
  Pallas kernels: 0 us -> 153 us
  waiting for transfers between devices: 123 us -> 0.07 us
  blocking collectives: 82.3 us -> 0 us
  matrix products: 34.9 us -> 21.8 us
  local copies, waits for them, and re-layouts: 47.9 us -> 35.4 us
  starting transfers between devices: 6 us -> 0.26 us
    pallas_call x0 -> x2, Pallas kernels: none -> 153 us  [the longest x1 86.9 us: moe_gather(): pl.pallas_call(lambda *refs: gather_kernel(ep_count, experts, width, *ref...]
    all_to_all x1 -> x0, blocking collectives: 55.6 us -> none  [local(): lax.all_to_all(outgoing, 'ep', split_axis=1, concat_axis=1, tiled=True)]
    all_to_all x1 -> x0, waiting for transfers between devices: 48 us -> none  [local(): lax.all_to_all(leaving, 'ep', split_axis=0, concat_axis=0, tiled=True)]
    all_gather x2 -> x1, waiting for transfers between devices: 43.4 us -> 0.02 us  [local(): gathered = lax.all_gather(packed, 'ep')]
    reduce_scatter x2 -> x1, waiting for transfers between devices: 31.7 us -> 0.02 us  [local(): lax.psum_scatter(mixer_part, 'tp', scatter_dimension=0, tiled=True)]
    all_gather x1 -> x0, blocking collectives: 26.6 us -> none  [prefix(): gathered = jax.tree.map(lambda a: lax.all_gather(a, axis), part)]
    dot_general x3 -> x0, matrix products: 14.6 us -> none  [the longest x1 6.45 us: local(): jnp.einsum('qsecd,edf->qsecf', shaped, w_gate, preferred_element_type=jnp...]
    convert_element_type x2 -> x0, local copies, waits for them, and re-layouts: 10 us -> none  [the longest x1 8.31 us: local(): projected.reshape(lax.axis_size('tp') * lane_rows, model_width)]
  transfers between devices with their start and end apart: 5 -> 2, of which waited for: 3 -> 0; matrix products, arithmetic and copies ran while one was open for 27% -> 3% of each run, Pallas kernels for 0% -> 64%
where the time goes in v1:
time: 241 us; the launch traced here: 240 us
  Pallas kernels  153 us (63%)
  local copies, waits for them, and re-layouts  35.4 us (15%)
  matrix products  21.8 us (9%)
  other arithmetic  14.6 us (6%)
  between operations  14.3 us (6%)
    pallas_call x1, Pallas kernels, moe_gather(): pl.pallas_call(lambda *refs: gather_kernel(ep_count, experts, width, *ref...  86.9 us
    pallas_call x1, Pallas kernels, moe_scatter(): pl.pallas_call(lambda *refs: scatter_kernel(count, *refs), out_shape=jax....  66.2 us
    dynamic_slice x24, local copies, waits for them, and re-layouts, local(): lax.scan(block_step, earlier_memory, (to_blocks(queries, head_count), to_...  15.9 us
    dot_general x8, matrix products, block_step(): jnp.einsum('htd,hde->hte', decayed_query, memory, precision=HIGHEST)  8.16 us
    dot_general x8, matrix products, block_step(): jnp.einsum('hsd,hse->hde', weight_block * jnp.exp(block_total - cumulativ...  5.35 us
  transfers between devices with their start and end apart: 2, of which 0 were waited for; matrix products, arithmetic and copies ran while one was open for 3% of the time, Pallas kernels for 64%

profile of v1, /device:TPU:0, one launch (start us, length us, event | category | flops | bytes accessed | tf_op | source)
XLA Modules:
  0.0 240.3 jit_solution(6269353034429315429)
XLA Ops:
  7.2 0.8 broadcast_subtract_fusion
  8.0 2.8 %negate_log-plus-one_fusion = (f32[512,512]{1,0:T(8,128)S(1)}, f32[512,512]{1,0:T(8,128)}) fusion(f32[512,512]{1,0:T(8,128)} %param.19, f32[512]{0:T(512)S(1)} %broadcast_subtract_fusion), kind=kLoop, calls=%fused_computation.43 | loop fusion | flops 1048576 | bytes 3147776 | tf_op jit(solution)/shard_map/log1p | solution.py:442
  10.9 0.7 fusion.21
  11.6 1.0 copy-done.2
  12.6 1.4 broadcast_add_fusion
  14.4 1.2 exponential_multiply_fusion
  15.6 2.6 %copy.88 = f32[512,512]{0,1:T(8,128)} copy(f32[512,512]{1,0:T(8,128)} %exponential_multiply_fusion) | data formatting | bytes 2097152 | tf_op jit(solution)/shard_map/reshape | solution.py:445
  18.4 1.5 fusion.13
  20.0 2.5 %fusion.15 = bf16[256,2048]{1,0:T(8,128)(2,1)} fusion(bf16[256,2048]{1,0:T(8,128)(2,1)} %param.25, f32[2048]{0:T(1024)S(1)} %copy-done.8, f32[256]{0:T(256)S(1)} %add_rsqrt_fusion), kind=kLoop, calls=%fused_computation.30 | loop fusion | flops 2097152 | bytes 2106368 | tf_op jit(solution)/shard_map/convert_element_type | solution.py:456
  22.5 3.0 %concatenate.9 = bf16[256,2176]{1,0:T(8,128)(2,1)} concatenate(bf16[256,2048]{1,0:T(8,128)(2,1)} %fusion.15, bf16[256,16]{1,0:T(8,128)(2,1)S(1)} %copy.74, bf16[256,16]{1,0:T(8,128)(2,1)S(1)} %copy.75, bf16[256,96]{1,0:T(8,128)(2,1)S(1)} %broadcast_in_dim.52), dimensions={1} | concatenate | bytes 2228224 | tf_op jit(solution)/shard_map/concatenate | solution.py:293
  25.5 2.5 %copy.76 = bf16[2,2,64,2176]{3,2,0,1:T(8,128)(2,1)} copy(bf16[2,2,64,2176]{3,2,1,0:T(8,128)(2,1)} %bitcast.115) | data formatting | bytes 2228224 | tf_op jit(solution)/shard_map/reshape | solution.py:295
  28.0 0.7 fusion.25
  28.7 0.7 pad_maximum_fusion
  29.7 1.3 reshape.114
  31.0 2.7 %reshape.115 = f32[8,64,4,128]{3,2,1,0:T(4,128)} reshape(f32[512,512]{1,0:T(8,128)} %get-tuple-element.134) | data formatting | bytes 2097152 | tf_op jit(solution)/shard_map/reshape | solution.py:48
  33.7 1.3 reshape.119
  35.0 1.3 reshape.120
  36.3 86.9 %moe_gather.1.refs_0_ = bf16[8,2,128,2048]{3,2,1,0:T(8,128)(2,1)} custom-call(bf16[2,128,2176]{2,1,0:T(8,128)(2,1)} %bitcast.123, bf16[2,2048,256]{2,1,0:T(8,128)(2,1)} %refs_1_.1, bf16[2,2048,256]{2,1,0:T(8,128)(2,1)} %refs_2_.1, bf16[2,256,2048]{2,1,0:T(8,128)(2,1)} %refs_3_.1), custom_call_target="tpu_custom_call" | custom-call | flops 12884901888 | bytes 104857600 | tf_op jit(solution)/shard_map/moe_gather/pallas_call | solution.py:307
  123.5 36.1 %while.23 = (s32[]{:T(128)}, f32[4,128,128]{2,1,0:T(8,128)S(1)}, f32[8,4,64,128]{3,2,1,0:T(8,128)}, f32[8,4,64,128]{3,1,2,0:T(4,128)}, f32[8,4,64,128]{3,1,2,0:T...) while((s32[]{:T(128)}, f32[4,128,128]{2,1,0:T(8,128)S(1)}, ...), condition=%wide.region_8.9_spmd, body=%wide.region_6.8_spmd.sunk | while | flops 153440256 | bytes 4084329 | solution.py:472
  123.5 1.0 constant_dynamic-slice_fusion.6
  124.7 1.0 constant_dynamic-slice_fusion.7
  125.7 0.4 convolution_select_fusion.2
  126.3 1.0 fusion.55
  127.3 0.7 convolution_add_fusion.3
  128.0 1.0 constant_dynamic-slice_fusion.6
  129.2 1.0 constant_dynamic-slice_fusion.7
  130.2 0.4 convolution_select_fusion.2
  130.8 1.0 fusion.55
  131.8 0.7 convolution_add_fusion.3
  132.5 1.0 constant_dynamic-slice_fusion.6
  133.7 1.0 constant_dynamic-slice_fusion.7
  134.7 0.4 convolution_select_fusion.2
  135.3 1.0 fusion.55
  136.3 0.7 convolution_add_fusion.3
  137.0 1.0 constant_dynamic-slice_fusion.6
  138.2 1.0 constant_dynamic-slice_fusion.7
  139.2 0.4 convolution_select_fusion.2
  139.8 1.0 fusion.55
  140.8 0.7 convolution_add_fusion.3
  141.5 1.0 constant_dynamic-slice_fusion.6
  142.7 1.0 constant_dynamic-slice_fusion.7
  143.7 0.4 convolution_select_fusion.2
  144.3 1.0 fusion.55
  145.4 0.7 convolution_add_fusion.3
  146.0 1.0 constant_dynamic-slice_fusion.6
  147.2 1.0 constant_dynamic-slice_fusion.7
  148.2 0.4 convolution_select_fusion.2
  148.8 1.0 fusion.55
  149.9 0.7 convolution_add_fusion.3
  150.6 1.0 constant_dynamic-slice_fusion.6
  151.7 1.0 constant_dynamic-slice_fusion.7
  153.3 1.0 fusion.55
  154.4 0.7 convolution_add_fusion.3
  155.1 1.0 constant_dynamic-slice_fusion.6
  156.2 1.0 constant_dynamic-slice_fusion.7
  157.2 0.4 convolution_select_fusion.2
  157.9 1.0 fusion.55
  158.9 0.7 convolution_add_fusion.3
  159.6 1.7 multiply_reduce_fusion
  161.4 0.7 copy.85
  162.1 0.6 mul.102
  162.7 2.7 %convolution_convert_fusion = bf16[512,2048]{1,0:T(8,128)(2,1)} fusion(bf16[512,2048]{1,0:T(8,128)(2,1)S(1)} %copy-done, bf16[512,512]{1,0:T(8,128)(2,1)S(1)} %copy-done.12, f32[64,8,4,128]{3,2,1,0:T(4,128)S(1)} %bitcast.124, f32[64,8,4,128]{3,2,1,0:T(4,128)S(1)} %bitcast.126, f32[512]{0:T(512)S(1)} %broadcast_bitcast_fusion), kind=kOutput, calls=%fused_computation.25 | convolution fusion | flops 1077149696 | bytes 6817792 | tf_op jit(solution)/shard_map/dot_general | solution.py:489
  165.5 66.2 %moe_scatter.1 = bf16[64,2048]{1,0:T(8,128)(2,1)} custom-call(bf16[8,2,128,2048]{3,2,1,0:T(8,128)(2,1)} %moe_gather.1.refs_0_), custom_call_target="tpu_custom_call" | custom-call | bytes 157286400 | tf_op jit(solution)/shard_map/moe_scatter/pallas_call | solution.py:335
  231.8 1.7 copy.166
  (98 shorter events, 5.3 us)
Async XLA Ops:
  7.2 155.6 %copy-start = (bf16[512,2048]{1,0:T(8,128)(2,1)S(1)}, bf16[512,2048]{1,0:T(8,128)(2,1)}, u32[]{:S(2)}) copy-start(bf16[512,2048]{1,0:T(8,128)(2,1)} %param.24) | copy-start | bytes 6291460
  7.2 116.0 %all-gather.3.cloned.1.call-start = ((), (), s32[]{:S(2)}) async-start(), calls=%async_computation.2 | async-start | bytes 2506752 | tf_op jit(solution)/shard_map/all_gather | solution.py:461
  11.5 1.0 copy-start.2
  12.6 1.8 copy-start.1
  14.4 3.8 %copy-start.9 = (f32[256,4]{0,1:T(4,128)S(1)}, f32[256,4]{0,1:T(4,128)}, u32[]{:S(2)}) copy-start(f32[256,4]{0,1:T(4,128)} %param.28) | copy-start | bytes 12292
  14.4 3.8 %copy-start.10 = (s32[256,4]{0,1:T(4,128)S(1)}, s32[256,4]{0,1:T(4,128)}, u32[]{:S(2)}) copy-start(s32[256,4]{0,1:T(4,128)} %param.27) | copy-start | bytes 12292
  15.6 4.4 %copy-start.8 = (f32[2048]{0:T(1024)S(1)}, f32[2048]{0:T(1024)}, u32[]{:S(2)}) copy-start(f32[2048]{0:T(1024)} %param.26) | copy-start | bytes 24580
  25.5 2.5 %copy-start.3 = (f32[512,512]{0,1:T(8,128)S(1)}, f32[512,512]{0,1:T(8,128)}, u32[]{:S(2)}) copy-start(f32[512,512]{0,1:T(8,128)} %copy.88) | copy-start | bytes 3145732
  25.5 2.5 %copy-start.5 = (bf16[512,512]{1,0:T(8,128)(2,1)S(1)}, bf16[512,512]{1,0:T(8,128)(2,1)}, u32[]{:S(2)}) copy-start(bf16[512,512]{1,0:T(8,128)(2,1)} %param.20) | copy-start | bytes 1572868
  29.4 202.4 %reduce-scatter.2.cloned.1.call-start = ((), (), s32[]{:S(2)}) async-start(), calls=%async_computation.1 | async-start | bytes 2621440 | tf_op jit(solution)/shard_map/reduce_scatter | solution.py:494
  31.0 2.7 %copy-start.6 = (bf16[512,512]{1,0:T(8,128)(2,1)S(1)}, bf16[512,512]{1,0:T(8,128)(2,1)}, u32[]{:S(2)}) copy-start(bf16[512,512]{1,0:T(8,128)(2,1)} %param.20) | copy-start | bytes 1572868
  31.0 4.0 %copy-start.7 = (bf16[512,512]{1,0:T(8,128)(2,1)S(1)}, bf16[512,512]{1,0:T(8,128)(2,1)}, u32[]{:S(2)}) copy-start(bf16[512,512]{1,0:T(8,128)(2,1)} %param.18) | copy-start | bytes 1572868
  33.7 2.6 %copy-start.11 = (f32[128]{0:T(128)S(1)}, f32[128]{0:T(128)}, u32[]{:S(2)}) copy-start(f32[128]{0:T(128)} %param.23) | copy-start | bytes 1540
  159.6 1.9 copy-start.4
  161.4 1.3 copy-start.12
Sparse Core Ops, SparseCore 0:
  29.6 73.6 all-gather.2
  165.6 37.7 reduce-scatter.1

commit v2 on v1

--- a/solution.py
+++ b/solution.py
@@ -15,39 +15,6 @@
 
 def rms_scale(values, gain):
     return values * lax.rsqrt(jnp.mean(values * values, axis=-1, keepdims=True) + EPS) * gain
-
-
-def block_step(memory, inputs):
-    queries_block, weight_block, values_block, forget_block = inputs
-    cumulative = jnp.cumsum(forget_block, axis=1)
-    length = queries_block.shape[1]
-    causal = (
-        jnp.arange(length, dtype=jnp.int32)[:, None] >= jnp.arange(length, dtype=jnp.int32)[None, :]
-    )
-    decayed_query = queries_block * jnp.exp(cumulative)
-    decayed_key = weight_block * jnp.exp(-cumulative)
-    carried_out = jnp.einsum("htd,hde->hte", decayed_query, memory, precision=HIGHEST)
-    scores = jnp.einsum("htd,hsd->hts", decayed_query, decayed_key, precision=HIGHEST)
-    scores = jnp.where(causal[None], scores, 0.0)
-    local_out = jnp.einsum("hts,hse->hte", scores, values_block, precision=HIGHEST)
-    block_total = cumulative[:, -1:, :]
-    added = jnp.einsum(
-        "hsd,hse->hde",
-        weight_block * jnp.exp(block_total - cumulative),
-        values_block,
-        precision=HIGHEST,
-    )
-    memory = jnp.exp(block_total[:, 0, :])[:, :, None] * memory + added
-    return (memory, carried_out + local_out)
-
-
-def to_blocks(array, head_count):
-    row_count = array.shape[0]
-    return (
-        array.astype(jnp.float32)
-        .reshape(row_count // BLOCK, BLOCK, head_count, HEAD_DIM)
-        .transpose(0, 2, 1, 3)
-    )
 
 
 def slot_ranks(ids_block, expert_count):
@@ -271,30 +238,150 @@
             hop(side, turn).wait_send()
 
 
-def dense_parts(normed, ids, weights, w_gate, w_up, w_down, ep_count):
-    rows, width = normed.shape
-    local_experts = w_gate.shape[0]
-    experts = local_experts * ep_count
-    half = rows // 2
-    routes = jnp.sum(
-        jnp.where(
-            ids[:, :, None] == jnp.arange(experts, dtype=jnp.int32)[None, None, :],
-            weights[:, :, None],
-            0.0,
-        ),
-        axis=1,
-    )
-    high = lax.reduce_precision(routes, 8, 7)
-    low = routes - high
+def contract(left, right, left_dim, right_dim):
+    return lax.dot_general(
+        left,
+        right,
+        (((left_dim,), (right_dim,)), ((), ())),
+        precision=HIGHEST,
+        preferred_element_type=jnp.float32,
+    )
+
+
+def decay_blocks(forget, bound):
+    weight = (1.0 - bound) * jax.nn.sigmoid(-forget)
+    logs = jnp.log1p(-weight)
+    lower = (
+        lax.broadcasted_iota(jnp.int32, (BLOCK, BLOCK), 0)
+        >= lax.broadcasted_iota(jnp.int32, (BLOCK, BLOCK), 1)
+    )
+    ones = jnp.where(lower, 1.0, 0.0)
+    blocks = []
+    for low in range(0, forget.shape[0], BLOCK):
+        cumulative = contract(ones, logs[low : low + BLOCK], 1, 0)
+        total = cumulative[BLOCK - 1 :]
+        blocks.append((weight[low : low + BLOCK], cumulative, total))
+    return lower, blocks
+
+
+def state_kernel(forget_ref, value_ref, bound_ref, out_ref):
+    _, blocks = decay_blocks(forget_ref[...], bound_ref[...])
+    memory, span = None, None
+    for at, (weight, cumulative, total) in enumerate(blocks):
+        values = value_ref[at * BLOCK : (at + 1) * BLOCK].astype(jnp.float32)
+        added = contract(values, weight * jnp.exp(total - cumulative), 0, 0)
+        memory = added if memory is None else memory * jnp.exp(total) + added
+        span = total if span is None else span + total
+    decay = jnp.broadcast_to(jnp.exp(span), (16, HEAD_DIM))
+    high = decay.astype(jnp.bfloat16).astype(jnp.float32)
+    first = lax.broadcasted_iota(jnp.int32, decay.shape, 0) < 8
+    out_ref[0, :HEAD_DIM] = memory.astype(jnp.bfloat16)
+    out_ref[0, HEAD_DIM:] = jnp.where(first, high, decay - high).astype(jnp.bfloat16)
+
+
+def mixer_kernel(
+    states_ref, query_ref, forget_ref, value_ref, gate_ref, bound_ref, gain_ref, out_ref
+):
+    def one(hop, memory):
+        tail = states_ref[hop, 0, HEAD_DIM:].astype(jnp.float32)
+        return memory * (tail[0:1] + tail[8:9]) + states_ref[hop, 0, :HEAD_DIM].astype(jnp.float32)
+
+    memory = lax.fori_loop(
+        0, lax.axis_index("ep"), one, jnp.zeros((HEAD_DIM, HEAD_DIM), jnp.float32)
+    )
+    lower, blocks = decay_blocks(forget_ref[...], bound_ref[...])
+    for at, (weight, cumulative, total) in enumerate(blocks):
+        rows = slice(at * BLOCK, (at + 1) * BLOCK)
+        values = value_ref[rows].astype(jnp.float32)
+        decayed_query = query_ref[rows].astype(jnp.float32) * jnp.exp(cumulative)
+        scores = contract(decayed_query, weight * jnp.exp(-cumulative), 1, 1)
+        result = contract(jnp.where(lower, scores, 0.0), values, 1, 0)
+        result += contract(decayed_query, memory, 1, 1)
+        added = contract(values, weight * jnp.exp(total - cumulative), 0, 0)
+        memory = memory * jnp.exp(total) + added
+        gate = jax.nn.silu(gate_ref[rows].astype(jnp.float32))
+        out_ref[rows] = (rms_scale(result, gain_ref[...]) * gate).astype(jnp.bfloat16)
+
+
+def head_block(rows):
+    return pl.BlockSpec((rows, HEAD_DIM), lambda head: (0, head))
+
+
+def head_states(forget_pre, value_in, lower_bound):
+    rows, width = forget_pre.shape
+    heads = width // HEAD_DIM
+    return pl.pallas_call(
+        state_kernel,
+        grid=(heads,),
+        out_shape=jax.ShapeDtypeStruct((heads, HEAD_DIM + 16, HEAD_DIM), jnp.bfloat16),
+        in_specs=[head_block(rows), head_block(rows), head_block(1)],
+        out_specs=pl.BlockSpec((1, HEAD_DIM + 16, HEAD_DIM), lambda head: (head, 0, 0)),
+        cost_estimate=pl.CostEstimate(
+            flops=10**9, bytes_accessed=8 * forget_pre.size, transcendentals=0
+        ),
+        name="head_states",
+    )(forget_pre, value_in, lower_bound[None])
+
+
+def mix_heads(states, queries, forget_pre, value_in, out_gate, lower_bound, out_gain):
+    rows, width = forget_pre.shape
+    heads = width // HEAD_DIM
+    count = states.shape[0]
+    return pl.pallas_call(
+        mixer_kernel,
+        grid=(heads,),
+        out_shape=jax.ShapeDtypeStruct((rows, width), jnp.bfloat16),
+        in_specs=[
+            pl.BlockSpec((count, 1, HEAD_DIM + 16, HEAD_DIM), lambda head: (0, head, 0, 0)),
+            head_block(rows),
+            head_block(rows),
+            head_block(rows),
+            head_block(rows),
+            head_block(1),
+            pl.BlockSpec((1, HEAD_DIM), lambda head: (0, 0)),
+        ],
+        out_specs=head_block(rows),
+        cost_estimate=pl.CostEstimate(
+            flops=4 * 10**9, bytes_accessed=16 * forget_pre.size, transcendentals=0
+        ),
+        name="mix_heads",
+    )(states, queries, forget_pre, value_in, out_gate, lower_bound[None], out_gain[None])
+
+
+def prepare_kernel(experts, token_ref, gain_ref, ids_ref, weights_ref, out_ref):
+    rows, width = token_ref.shape
+    normed = rms_scale(token_ref[...].astype(jnp.float32), gain_ref[...]).astype(jnp.bfloat16)
+    margin = out_ref.shape[2] - width
+    column = lax.broadcasted_iota(jnp.int32, (rows, margin), 1)
+    extra = jnp.zeros((rows, margin), jnp.float32)
+    for choice in range(ids_ref.shape[1]):
+        number = ids_ref[:, choice : choice + 1]
+        weight = weights_ref[:, choice : choice + 1]
+        high = weight.astype(jnp.bfloat16).astype(jnp.float32)
+        extra += jnp.where(column == number, high, 0.0)
+        extra += jnp.where(column == number + experts, weight - high, 0.0)
+    extra = extra.astype(jnp.bfloat16)
+    step = rows // 4
+    for core in range(2):
+        for cross in range(2):
+            low = (2 * cross + core) * step
+            out_ref[core, cross * step : (cross + 1) * step, :width] = normed[low : low + step]
+            out_ref[core, cross * step : (cross + 1) * step, width:] = extra[low : low + step]
+
+
+def prepare(tokens, gain, ids, weights, experts):
+    rows, width = tokens.shape
     margin = -(-2 * experts // 128) * 128
-    extra = jnp.concatenate(
-        [high, low, jnp.zeros((rows, margin - 2 * experts), jnp.float32)], axis=1
-    ).astype(jnp.bfloat16)
-    full = jnp.concatenate([normed, extra], axis=1)
-    stride = width + margin
-    full = full.reshape(2, 2, half // 2, stride).transpose(1, 0, 2, 3).reshape(2, half, stride)
-    turns = ep_count // 2
-    return full, margin, half, turns, experts
+    return pl.pallas_call(
+        lambda *refs: prepare_kernel(experts, *refs),
+        out_shape=jax.ShapeDtypeStruct((2, rows // 2, width + margin), jnp.bfloat16),
+        in_specs=[VMEM] * 4,
+        out_specs=VMEM,
+        cost_estimate=pl.CostEstimate(
+            flops=10**6, bytes_accessed=4 * tokens.size, transcendentals=0
+        ),
+        name="prepare",
+    )(tokens, gain[None], ids, weights)
 
 
 def moe_gather(full, w_gate, w_up, w_down, ep_count, experts):
@@ -435,56 +522,21 @@
 ):
     lanes = lax.axis_size("tp")
     ep_count = lax.axis_size("ep")
-    seq_rows, local_width = queries.shape
     model_width = out_weight.shape[1]
-    head_count = local_width // HEAD_DIM
-    weight_in = (1.0 - lower_bound) * jax.nn.sigmoid(-forget_pre)
-    log_forget = jnp.log1p(-weight_in)
-    cumulative = jnp.cumsum(log_forget, axis=0)
-    span_total = cumulative[-1]
-    to_end = (weight_in * jnp.exp(span_total[None, :] - cumulative)).reshape(
-        seq_rows, head_count, HEAD_DIM
-    )
-    values_float = value_in.astype(jnp.float32).reshape(seq_rows, head_count, HEAD_DIM)
-    local_memory = jnp.einsum("shd,she->hde", to_end, values_float, precision=HIGHEST)
-    decay_total = jnp.exp(span_total).reshape(head_count, HEAD_DIM)
-    packed = jnp.concatenate([local_memory, decay_total[:, None, :]], axis=1)
+    packed = head_states(forget_pre, value_in, lower_bound)
     tokens, top_count = expert_ids.shape
     dense_slots = 2 * (tokens // lanes) * top_count * lanes
     dense = lanes == 4 and ep_count % 2 == 0 and tokens * ep_count <= dense_slots
     if dense:
-        normed = rms_scale(moe_tokens.astype(jnp.float32), moe_gain).astype(jnp.bfloat16)
-        full, _, _, _, experts = dense_parts(
-            normed, expert_ids, route_weights, w_gate, w_up, w_down, ep_count
-        )
+        experts = w_gate.shape[0] * ep_count
+        full = prepare(moe_tokens, moe_gain, expert_ids, route_weights, experts)
         full, packed = lax.optimization_barrier((full, packed))
     gathered = lax.all_gather(packed, "ep")
     if dense:
         parts = moe_gather(full, w_gate, w_up, w_down, ep_count, experts)
         gathered, parts = lax.optimization_barrier((gathered, parts))
-    place = lax.axis_index("ep")
-
-    def one(hop, state):
-        block = lax.dynamic_index_in_dim(gathered, hop, 0, False)
-        return block[:, HEAD_DIM:, :].reshape(head_count, HEAD_DIM, 1) * state + block[:, :HEAD_DIM]
-
-    earlier_memory = lax.fori_loop(0, place, one, jnp.zeros_like(local_memory))
-    final_memory, outputs = lax.scan(
-        block_step,
-        earlier_memory,
-        (
-            to_blocks(queries, head_count),
-            to_blocks(weight_in, head_count),
-            to_blocks(value_in, head_count),
-            to_blocks(log_forget, head_count),
-        ),
-    )
-    outputs = outputs.transpose(0, 2, 1, 3).reshape(seq_rows, head_count, HEAD_DIM)
-    gate_act = jax.nn.silu(out_gate.astype(jnp.float32)).reshape(seq_rows, head_count, HEAD_DIM)
-    gated = (
-        (rms_scale(outputs, out_gain) * gate_act)
-        .reshape(seq_rows, local_width)
-        .astype(jnp.bfloat16)
+    gated = mix_heads(
+        gathered, queries, forget_pre, value_in, out_gate, lower_bound, out_gain
     )
     mixer_part = jnp.dot(gated, out_weight, preferred_element_type=jnp.float32).astype(
         jnp.bfloat16

time: 241 us -> 180 us (0.75)
  local copies, waits for them, and re-layouts: 35.4 us -> 4.78 us
  matrix products: 21.8 us -> 3.65 us
  other arithmetic: 14.6 us -> 0 us
  Pallas kernels: 153 us -> 157 us
    pallas_call x0 -> x3, Pallas kernels: none -> 21.1 us  [the longest x1 12.7 us: mix_heads(): pl.pallas_call(mixer_kernel, grid=(heads,), out_shape=jax.ShapeDtypeStruc...]
    dot_general x33 -> x0, matrix products: 19.1 us -> none  [the longest x8 8.16 us: block_step(): jnp.einsum('htd,hde->hte', decayed_query, memory, precision=HIGHEST)]
    dynamic_slice x24 -> x0, local copies, waits for them, and re-layouts: 15.9 us -> none  [local(): lax.scan(block_step, earlier_memory, (to_blocks(queries, head_count), to_...]
    pallas_call x1, Pallas kernels: 86.9 us -> 72.2 us  [moe_gather(): pl.pallas_call(lambda *refs: gather_kernel(ep_count, experts, width, *ref...]
    reshape x4 -> x0, local copies, waits for them, and re-layouts: 9.04 us -> none  [the longest x2 4.03 us: to_blocks(): return array.astype(jnp.float32).reshape(row_count // BLOCK, BLOCK, head_...]
    transpose x3 -> x0, local copies, waits for them, and re-layouts: 3.28 us -> none  [the longest x2 2.6 us: to_blocks(): return array.astype(jnp.float32).reshape(row_count // BLOCK, BLOCK, head_...]
    another operation x12 -> x0, other arithmetic: 3.24 us -> none
    reduce_sum x3 -> x0, other arithmetic: 3.18 us -> none  [the longest x2 3.17 us: rms_scale(): jnp.mean(values * values, axis=-1, keepdims=True) + EPS]
  transfers between devices with their start and end apart: 2 -> 2, of which waited for: 0 -> 0; matrix products, arithmetic and copies ran while one was open for 3% -> 0% of each run, Pallas kernels for 64% -> 76%
where the time goes in v2:
time: 180 us
  Pallas kernels  157 us (87%)
  between operations  14.1 us (8%)
  local copies, waits for them, and re-layouts  4.78 us (3%)
  matrix products  3.65 us (2%)
    pallas_call x1, Pallas kernels, moe_gather(): pl.pallas_call(lambda *refs: gather_kernel(ep_count, experts, width, *ref...  72.2 us
    pallas_call x1, Pallas kernels, moe_scatter(): pl.pallas_call(lambda *refs: scatter_kernel(count, *refs), out_shape=jax....  63.7 us
    pallas_call x1, Pallas kernels, mix_heads(): pl.pallas_call(mixer_kernel, grid=(heads,), out_shape=jax.ShapeDtypeStruc...  12.7 us
    pallas_call x1, Pallas kernels, head_states(): pl.pallas_call(state_kernel, grid=(heads,), out_shape=jax.ShapeDtypeStruc...  5.19 us
    unnamed x5, local copies, waits for them, and re-layouts  4.78 us
    dot_general x1, matrix products, local(): jnp.dot(gated, out_weight, preferred_element_type=jnp.float32)  3.65 us
  transfers between devices with their start and end apart: 2, of which 0 were waited for; matrix products, arithmetic and copies ran while one was open for 0% of the time, Pallas kernels for 76%

profile of v2, /device:TPU:0, one launch (start us, length us, event | category | flops | bytes accessed | tf_op | source)
XLA Modules:
  0.0 179.7 jit_solution(1599949037729198133)
XLA Ops:
  7.2 0.0 copy-start
  7.2 0.0 all-gather.3.cloned.1.call-start
  7.2 1.6 copy.18.refs_2_
  8.8 1.5 copy.19.refs_3_
  10.3 5.2 %head_states.1 = bf16[4,144,128]{2,1,0:T(8,128)(2,1)} custom-call(f32[512,512]{1,0:T(8,128)} %forget_ref.3, bf16[512,512]{1,0:T(8,128)(2,1)} %value_ref.3, f32[1,512]{1,0:T(1,128)} %bitcast.8), custom_call_target="tpu_custom_call" | custom-call | flops 1000000000 | bytes 2097152 | tf_op jit(solution)/shard_map/head_states/pallas_call | solution.py:313
  15.5 3.2 %prepare.1.refs_0_ = bf16[2,128,2176]{2,1,0:T(8,128)(2,1)} custom-call(bf16[256,2048]{1,0:T(8,128)(2,1)} %refs_0_.1, f32[1,2048]{1,0:T(1,128)} %bitcast.6, s32[256,4]{1,0:T(8,128)} %copy.18.refs_2_, f32[256,4]{1,0:T(8,128)} %copy.19.refs_3_), custom_call_target="tpu_custom_call" | custom-call | flops 1000000 | bytes 2097152 | tf_op jit(solution)/shard_map/prepare/pallas_call | solution.py:375
  18.7 0.0 all-gather.3.cloned.1.call-update
  18.7 0.0 reduce-scatter.2.cloned.1.call-start
  18.8 72.2 %moe_gather.1.refs_0_ = bf16[8,2,128,2048]{3,2,1,0:T(8,128)(2,1)} custom-call(bf16[2,128,2176]{2,1,0:T(8,128)(2,1)} %prepare.1.refs_0_, bf16[2,2048,256]{2,1,0:T(8,128)(2,1)} %refs_1_.1, bf16[2,2048,256]{2,1,0:T(8,128)(2,1)} %refs_2_.2, bf16[2,256,2048]{2,1,0:T(8,128)(2,1)} %refs_3_.2), custom_call_target="tpu_custom_call" | custom-call | flops 12884901888 | bytes 104857600 | tf_op jit(solution)/shard_map/moe_gather/pallas_call | solution.py:394
  91.0 0.0 all-gather.3.cloned.1.call-done
  91.1 12.7 %mix_heads.1 = bf16[512,512]{1,0:T(8,128)(2,1)} custom-call(bf16[8,4,144,128]{3,2,1,0:T(8,128)(2,1)} %bitcast.7, bf16[512,512]{1,0:T(8,128)(2,1)} %query_ref.1, f32[512,512]{1,0:T(8,128)} %forget_ref.3, bf16[512,512]{1,0:T(8,128)(2,1)} %value_ref.3, bf16[512,512]{1,0:T(8,128)(2,1)} %gate_ref.1, f32[1,512]{1,0:T(1,128)} %bitcast.9, f32[1,128]{1,0:T(1,128)} %bitcast.10), custom_call_target="tpu_custom_call" | custom-call | flops 4000000000 | bytes 4194304 | tf_op jit(solution)/shard_map/mix_heads/pallas_call | solution.py:330
  103.8 0.0 copy-done
  103.8 3.7 %convolution_convert_fusion = bf16[512,2048]{1,0:T(8,128)(2,1)} fusion(bf16[512,512]{1,0:T(8,128)(2,1)} %mix_heads.1, bf16[512,2048]{1,0:T(8,128)(2,1)S(1)} %copy-done), kind=kOutput, calls=%fused_computation | convolution fusion | flops 1074790400 | bytes 4718592 | tf_op jit(solution)/shard_map/dot_general | solution.py:541
  107.4 0.0 reduce-scatter.2.cloned.1.call-update
  107.4 63.7 %moe_scatter.1 = bf16[64,2048]{1,0:T(8,128)(2,1)} custom-call(bf16[8,2,128,2048]{3,2,1,0:T(8,128)(2,1)} %moe_gather.1.refs_0_), custom_call_target="tpu_custom_call" | custom-call | bytes 157286400 | tf_op jit(solution)/shard_map/moe_scatter/pallas_call | solution.py:422
  171.1 0.0 reduce-scatter.2.cloned.1.call-done
  171.1 1.7 copy.21
Async XLA Ops:
  7.2 96.6 %copy-start = (bf16[512,2048]{1,0:T(8,128)(2,1)S(1)}, bf16[512,2048]{1,0:T(8,128)(2,1)}, u32[]{:S(2)}) copy-start(bf16[512,2048]{1,0:T(8,128)(2,1)} %param.20) | copy-start | bytes 6291460
  7.2 83.9 %all-gather.3.cloned.1.call-start = ((), (), s32[]{:S(2)}) async-start(), calls=%async_computation.2 | async-start | bytes 1327104 | tf_op jit(solution)/shard_map/all_gather | solution.py:534
  18.7 152.4 %reduce-scatter.2.cloned.1.call-start = ((), (), s32[]{:S(2)}) async-start(), calls=%async_computation.1 | async-start | bytes 2621440 | tf_op jit(solution)/shard_map/reduce_scatter | solution.py:546
Sparse Core Ops, SparseCore 0:
  18.9 50.6 all-gather.2
  107.6 33.7 reduce-scatter.1
